TPU v7x, 32 devices: a whole 2x2x4 slice. The times are simulated.
32 devices in a mesh: sp: 8 (over z, y), tp: 4 (over x, core).
Axes of the slice: x: 2, y: 2, z: 4, core: 2. Of those that a mesh axis runs over, the one named last changes fastest.
Arguments:
- stream: bfloat16 [2048, 2048], P(('sp', 'tp')), may hold values from -6 to 6
- queries: bfloat16 [2048, 2048], P('sp', 'tp'), may hold values from -147.07821 to 147.07821
- keys: bfloat16 [2048, 2048], P('sp', 'tp'), may hold values from -7 to 7
- values: bfloat16 [2048, 2048], P('sp', 'tp'), may hold values from -6 to 6
- head_lambda: float32 [8], P('tp'), may hold values from 0.3 to 0.8
- head_gain: float32 [256], replicated, may hold values from 0.1 to 1.9
- w_out: bfloat16 [2048, 2048], P('tp'), may hold values from -0.125 to 0.125
- norm_gain: float32 [2048], replicated, may hold values from 0.1 to 1.9
- w_gate: bfloat16 [2048, 5632], P('sp', 'tp'), may hold values from -0.125 to 0.125
- w_up: bfloat16 [2048, 5632], P('sp', 'tp'), may hold values from -0.125 to 0.125
- w_down: bfloat16 [5632, 2048], P('tp', 'sp'), may hold values from -0.078125 to 0.078125
Outputs:
- result: bfloat16 [2048, 2048], P(('sp', 'tp'))
All inputs are finite; a program needn't handle non-finite values.
Results may differ from a plain program's by a relative error of at most 0.013.
Values may be sent and summed in bfloat16 or wider, within the bound.
A program may use at most 192 MiB of HBM per device.

v0:
```python
import jax
import jax.numpy as jnp
from jax import lax
from jax.sharding import PartitionSpec as P

epsilon = 1e-06


def normalize(values_in, gain):
    square_mean = jnp.mean(values_in * values_in, axis=-1, keepdims=True)
    return values_in * lax.rsqrt(square_mean + epsilon) * gain


def shards(
    stream, queries, keys, values, head_lambda, head_gain, w_out, norm_gain, w_gate, w_up, w_down
):
    row_count = queries.shape[0]
    head_count = head_lambda.shape[0]
    head_dim = queries.shape[1] // (2 * head_count)
    value_dim = values.shape[1] // head_count
    score_scale = head_dim ** (-0.5)
    offset = lax.axis_index("sp") * row_count
    query_heads = queries.reshape(row_count, head_count, 2, head_dim)
    query_pos = offset + jnp.arange(row_count, dtype=jnp.int32)
    start_state = (
        jnp.full((head_count, 2, row_count), -1e30, jnp.float32),
        jnp.zeros((head_count, 2, row_count), jnp.float32),
        jnp.zeros((head_count, 2, row_count, value_dim), jnp.float32),
    )
    key_piece = lax.all_gather(keys, "sp", axis=0, tiled=True)
    value_piece = lax.all_gather(values, "sp", axis=0, tiled=True)
    span = key_piece.shape[0]

    def update(state):
        row_max, weight_sum, partial_value = state
        key_heads = key_piece.reshape(span, head_count, 2, head_dim)
        value_heads = value_piece.reshape(span, head_count, value_dim)
        scores = (
            jnp.einsum(
                "qhsd,khsd->hsqk", query_heads, key_heads, preferred_element_type=jnp.float32
            )
            * score_scale
        )
        key_pos = jnp.arange(span, dtype=jnp.int32)
        visible = key_pos[None, :] <= query_pos[:, None]
        new_max = jnp.maximum(row_max, jnp.max(jnp.where(visible, scores, -1e30), axis=-1))
        weights = jnp.where(visible, jnp.exp(scores - new_max[..., None]), 0.0)
        new_sum = jnp.sum(weights, axis=-1)
        added = jnp.einsum(
            "hsqk,khd->hsqd",
            weights.astype(jnp.bfloat16),
            value_heads,
            preferred_element_type=jnp.float32,
        )
        return (new_max, new_sum, added)

    def unchanged(state):
        return state

    row_max, weight_sum, partial_value = lax.cond(
        jnp.int32(0) <= offset + row_count - 1, update, unchanged, start_state
    )
    map_out = partial_value / weight_sum[..., None]
    contrast = map_out[:, 0] - head_lambda[:, None, None] * map_out[:, 1]
    head_out = (
        normalize(contrast, head_gain)
        .transpose(1, 0, 2)
        .reshape(row_count, head_count * value_dim)
        .astype(jnp.bfloat16)
    )
    local_rows = stream.shape[0]
    projected = lax.psum(
        jnp.dot(head_out, w_out, preferred_element_type=jnp.float32).astype(jnp.bfloat16), "tp"
    ).astype(jnp.float32)
    stream_all = lax.all_gather(stream, "tp", axis=0, tiled=True)
    middle_all = stream_all.astype(jnp.float32) + projected
    mixer_in = normalize(middle_all, norm_gain).astype(jnp.bfloat16)
    middle = lax.dynamic_slice_in_dim(middle_all, lax.axis_index("tp") * local_rows, local_rows, 0)
    gate = jnp.dot(
        mixer_in,
        lax.all_gather(w_gate, "sp", axis=0, tiled=True),
        preferred_element_type=jnp.float32,
    )
    up_part = jnp.dot(
        mixer_in, lax.all_gather(w_up, "sp", axis=0, tiled=True), preferred_element_type=jnp.float32
    )
    down_full = lax.all_gather(w_down, "sp", axis=1, tiled=True)
    hidden = (jax.nn.silu(gate) * up_part).astype(jnp.bfloat16)
    mixed = lax.psum_scatter(
        jnp.dot(hidden, down_full, preferred_element_type=jnp.float32).astype(jnp.bfloat16),
        "tp",
        scatter_dimension=0,
        tiled=True,
    ).astype(jnp.float32)
    return (middle + mixed).astype(jnp.bfloat16)


def solution(mesh):
    placed = (
        P(("sp", "tp"), None),
        P("sp", "tp"),
        P("sp", "tp"),
        P("sp", "tp"),
        P("tp"),
        P(),
        P("tp", None),
        P(),
        P("sp", "tp"),
        P("sp", "tp"),
        P("tp", "sp"),
    )
    return jax.shard_map(
        shards, mesh=mesh, in_specs=placed, out_specs=P(("sp", "tp"), None), check_vma=False
    )
```

profile of v0, /device:TPU:0, one launch (start us, length us, event | category | flops | bytes accessed | tf_op | source)
XLA Modules:
  0.0 499.6 jit_solution(3734772541105203988)
XLA Ops:
  6.5 0.7 all-gather.11.cloned.1.call-update
  7.3 0.7 all-gather.9.cloned.1.call-update
  8.1 0.7 all-gather.7.cloned.1.call-update
  8.8 52.5 %all-gather.11.cloned.1.call-done = bf16[2048,512]{1,0:T(8,128)(2,1)} async-done(((bf16[256,512]{1,0:T(8,128)(2,1)}), bf16[2048,512]{1,0:T(8,128)(2,1)}) %all-gather.11.cloned.1.call-update) | async-done | bytes 2097168 | tf_op jit(solution)/shard_map/all_gather | solution.py:31
  61.3 49.8 %all-gather.9.cloned.1.call-done = bf16[2048,512]{1,0:T(8,128)(2,1)} async-done(((bf16[256,512]{1,0:T(8,128)(2,1)}), bf16[2048,512]{1,0:T(8,128)(2,1)}) %all-gather.9.cloned.1.call-update) | async-done | bytes 2097168 | tf_op jit(solution)/shard_map/all_gather | solution.py:30
  111.1 28.6 %conditional.1 = (f32[2,2,256]{2,1,0:T(2,128)S(1)}, f32[2,2,256,256]{2,3,0,1:T(8,128)S(1)}) conditional(s32[]{:T(128)} %convert_element_type.40, () %tuple.13, (s32[]{:T(128)}, s32[256]{0:T(256)S(1)}, bf16[256,512]{1,0:T(8,128)(2,1)}, bf16[2048,512]{1,0:T(8,128)(2,1)}, bf16[2048,512]{1,0:T(8,128)(2,1)}) %tuple.14), branch_computations={%region_0.0_spmd, %region_1.4_spmd} | conditional | flops 1634204928 | bytes 46951500 | solution.py:60
  111.5 4.2 reshape.34
  115.8 6.8 %select_reduce_fusion = (f32[2,2,256]{2,1,0:T(2,128)S(1)}, f32[2,2,256,2048]{3,2,1,0:T(8,128)}) fusion(pred[256,2048]{1,0:T(8,128)(4,1)S(1)} %iota_compare_fusion, bf16[2048,2,2,128]{3,2,1,0:T(2,128)(2,1)} %reshape.34, bf16[256,2,2,128]{3,2,1,0:T(2,128)(2,1)S(1)} %reshape.33), kind=kOutput, calls=%fused_computation.1 | convolution fusion | flops 543161344 | bytes 11276288 | tf_op jit(solution)/shard_map/cond/branch_1_fun/qhsd,khsd->hsqk/dot_general | solution.py:39
  122.6 4.0 reshape.35
  126.6 6.8 %fusion.2 = f32[2,2,256,256]{3,2,1,0:T(8,128)} fusion(f32[2,2,256,2048]{3,2,1,0:T(8,128)} %get-tuple-element.31, f32[2,2,256]{2,1,0:T(2,128)S(1)} %broadcast_maximum_fusion, pred[256,2048]{1,0:T(8,128)(4,1)S(1)} %iota_compare_fusion, bf16[2048,2,256,1]{2,1,0,3:T(2,128)(2,1)} %bitcast.27), kind=kOutput, calls=%fused_computation.4 | convolution fusion | flops 1082130432 | bytes 12062720 | tf_op jit(solution)/shard_map/cond/branch_1_fun/hsqk,khd->hsqd/dot_general | solution.py:49
  133.4 1.6 copy.26
  134.9 4.7 fusion.1
  140.6 1.7 convolution_convert_fusion
  142.4 0.5 all-gather.13.cloned.1.call-update
  143.6 0.7 all-gather.17.cloned.1.call-update
  144.6 32.8 %all-reduce.2.cloned.1.call-done = bf16[256,2048]{1,0:T(8,128)(2,1)} async-done(((bf16[256,2048]{1,0:T(8,128)(2,1)}), bf16[256,2048]{1,0:T(8,128)(2,1)}) %all-reduce.2.cloned.1.call-update) | async-done | bytes 1048592 | tf_op jit(solution)/shard_map/psum | solution.py:72
  177.3 3.2 convert_add_fusion
  180.6 91.6 %all-gather.13.cloned.1.call-done = bf16[2048,1408]{1,0:T(8,128)(2,1)} async-done(((bf16[256,1408]{1,0:T(8,128)(2,1)}), bf16[2048,1408]{1,0:T(8,128)(2,1)}) %all-gather.13.cloned.1.call-update) | async-done | bytes 5767184 | tf_op jit(solution)/shard_map/all_gather | solution.py:81
  272.2 5.9 %fusion.18 = f32[256,1408]{1,0:T(8,128)} fusion(bf16[2048,1408]{1,0:T(8,128)(2,1)} %all-gather.13.cloned.1.call-done, f32[2048]{0:T(1024)S(1)} %copy-done.6, f32[256]{0:T(256)S(1)} %add_rsqrt_fusion.1, bf16[256,2048]{1,0:T(8,128)(2,1)} %all-reduce.2.cloned.1.call-done, bf16[256,2048]{1,0:T(8,128)(2,1)S(1)} %copy-done.2), kind=kOutput, calls=%fused_computation.36 | convolution fusion | flops 1479540736 | bytes 9315328 | tf_op jit(solution)/shard_map/dot_general | solution.py:79
  278.1 86.6 %all-gather.15.cloned.1.call-done = bf16[2048,1408]{1,0:T(8,128)(2,1)} async-done(((bf16[256,1408]{1,0:T(8,128)(2,1)}), bf16[2048,1408]{1,0:T(8,128)(2,1)}) %all-gather.15.cloned.1.call-update) | async-done | bytes 5767184 | tf_op jit(solution)/shard_map/all_gather | solution.py:85
  364.8 93.4 %all-gather.17.cloned.1.call-done = bf16[1408,2048]{1,0:T(8,128)(2,1)} async-done(((bf16[1408,256]{1,0:T(8,128)(2,1)}), bf16[1408,2048]{1,0:T(8,128)(2,1)}) %all-gather.17.cloned.1.call-update) | async-done | bytes 5767184 | tf_op jit(solution)/shard_map/all_gather | solution.py:87
  458.1 9.6 %convolution_convert_fusion.1 = bf16[256,2048]{1,0:T(8,128)(2,1)} fusion(bf16[1408,2048]{1,0:T(8,128)(2,1)} %all-gather.17.cloned.1.call-done, bf16[2048,1408]{1,0:T(8,128)(2,1)} %all-gather.15.cloned.1.call-done, f32[256,1408]{1,0:T(8,128)} %fusion.18, f32[2048]{0:T(1024)S(1)} %copy-done.6, f32[256]{0:T(256)S(1)} %add_rsqrt_fusion.1, ...), kind=kOutput, calls=%fused_computation.21 | convolution fusion | flops 2958622720 | bytes 16131072 | tf_op jit(solution)/shard_map/dot_general | solution.py:90
  467.8 23.1 %reduce-scatter.2.cloned.1.call-done = bf16[64,2048]{1,0:T(8,128)(2,1)} async-done(((bf16[256,2048]{1,0:T(8,128)(2,1)}), bf16[64,2048]{1,0:T(8,128)(2,1)}) %reduce-scatter.2.cloned.1.call-update) | async-done | bytes 262160 | tf_op jit(solution)/shard_map/reduce_scatter | solution.py:89
  490.9 1.9 add_convert_fusion
  (37 shorter events, 2.4 us)
Async XLA Ops:
  6.5 134.1 %copy-start = (bf16[512,2048]{1,0:T(8,128)(2,1)S(1)}, bf16[512,2048]{1,0:T(8,128)(2,1)}, u32[]{:S(2)}) copy-start(bf16[512,2048]{1,0:T(8,128)(2,1)} %param.19) | copy-start | bytes 6291460
  6.5 54.8 %all-gather.11.cloned.1.call-start = ((), (), s32[]{:S(2)}) async-start(), calls=%async_computation.3 | async-start | bytes 2359296 | tf_op jit(solution)/shard_map/all_gather | solution.py:31
  7.3 103.8 %all-gather.9.cloned.1.call-start = ((), (), s32[]{:S(2)}) async-start(), calls=%async_computation.2 | async-start | bytes 2359296 | tf_op jit(solution)/shard_map/all_gather | solution.py:30
  8.0 136.6 %all-gather.7.cloned.1.call-start = ((), (), s32[]{:S(2)}) async-start(), calls=%async_computation.1 | async-start | bytes 1310720 | tf_op jit(solution)/shard_map/all_gather | solution.py:75
  8.7 168.6 %all-reduce.2.cloned.1.call-start = ((), (), s32[]{:S(2)}) async-start(), calls=%async_computation.4 | async-start | bytes 2097152 | tf_op jit(solution)/shard_map/psum | solution.py:72
  111.5 15.2 %copy-start.1 = (pred[256,2048]{1,0:T(8,128)(4,1)}, pred[256,2048]{1,0:T(8,128)(4,1)S(1)}, u32[]{:S(2)}) copy-start(pred[256,2048]{1,0:T(8,128)(4,1)S(1)} %iota_compare_fusion) | copy-start | bytes 1572868 | tf_op jit(solution)/shard_map/cond
  111.5 4.2 copy-start.3
  139.6 0.7 copy-start.4
  139.7 0.8 copy-start.5
  142.4 129.8 %all-gather.13.cloned.1.call-start = ((), (), s32[]{:S(2)}) async-start(), calls=%async_computation.5 | async-start | bytes 6488064 | tf_op jit(solution)/shard_map/all_gather | solution.py:81
  143.0 221.8 %all-gather.15.cloned.1.call-start = ((), (), s32[]{:S(2)}) async-start(), calls=%async_computation.6 | async-start | bytes 6488064 | tf_op jit(solution)/shard_map/all_gather | solution.py:85
  143.6 314.6 %all-gather.17.cloned.1.call-start = ((), (), s32[]{:S(2)}) async-start(), calls=%async_computation.7 | async-start | bytes 6488064 | tf_op jit(solution)/shard_map/all_gather | solution.py:87
  144.3 127.9 %copy-start.6 = (f32[2048]{0:T(1024)S(1)}, f32[2048]{0:T(1024)}, u32[]{:S(2)}) copy-start(f32[2048]{0:T(1024)} %param.20) | copy-start | bytes 24580
  144.3 346.6 %reduce-scatter.2.cloned.1.call-start = ((), (), s32[]{:S(2)}) async-start(), calls=%async_computation.8 | async-start | bytes 1310720 | tf_op jit(solution)/shard_map/reduce_scatter | solution.py:89
  144.6 127.6 %copy-start.2 = (bf16[256,2048]{1,0:T(8,128)(2,1)S(1)}, bf16[256,2048]{1,0:T(8,128)(2,1)}, u32[]{:S(2)}) copy-start(bf16[256,2048]{1,0:T(8,128)(2,1)} %all-gather.7.cloned.1.call-done) | copy-start | bytes 3145732
Sparse Core Ops, SparseCore 0:
  9.5 51.7 all-gather.10
  63.4 47.6 all-gather.8
  112.6 15.2 all-gather.6
  142.5 34.7 all-reduce.1
  179.4 92.7 all-gather.12
  274.2 90.4 all-gather.14
  366.8 91.2 all-gather.16
  467.9 22.9 reduce-scatter.1
where the time goes:
time: 500 us
  waiting for transfers between devices  434 us (87%)
  matrix products  30.9 us (6%)
  between operations  13.6 us (3%)
  other arithmetic  10.6 us (2%)
  local copies, waits for them, and re-layouts  10.4 us (2%)
    all_gather x1, waiting for transfers between devices, shards(): down_full = lax.all_gather(w_down, 'sp', axis=1, tiled=True)  93.4 us
    all_gather x1, waiting for transfers between devices, shards(): lax.all_gather(w_gate, 'sp', axis=0, tiled=True)  91.6 us
    all_gather x1, waiting for transfers between devices, shards(): lax.all_gather(w_up, 'sp', axis=0, tiled=True)  86.6 us
    all_gather x1, waiting for transfers between devices, shards(): value_piece = lax.all_gather(values, 'sp', axis=0, tiled=True)  52.5 us
    all_gather x1, waiting for transfers between devices, shards(): key_piece = lax.all_gather(keys, 'sp', axis=0, tiled=True)  49.8 us
    psum x1, waiting for transfers between devices, shards(): lax.psum(jnp.dot(head_out, w_out, preferred_element_type=jnp.float32).ast...  32.8 us
    reduce_scatter x1, waiting for transfers between devices, shards(): lax.psum_scatter(jnp.dot(hidden, down_full, preferred_element_type=jnp.fl...  23.1 us
  transfers between devices with their start and end apart: 8, of which 7 were waited for; matrix products, arithmetic and copies ran while one was open for 8% of the time, Pallas kernels for 0%

commit v1 on v0

v1 whole, which is shorter than its diff:
```python
import functools

import jax
import jax.numpy as jnp
from jax import lax
from jax.experimental import pallas as pl
from jax.experimental.pallas import tpu as pltpu
from jax.sharding import PartitionSpec as P

epsilon = 1e-06
MESH = pl.DeviceIdType.MESH
LANES = 128


def remote(src, dst, send_sem, recv_sem, sp, tp):
    return pltpu.make_async_remote_copy(
        src_ref=src,
        dst_ref=dst,
        send_sem=send_sem,
        recv_sem=recv_sem,
        device_id={"sp": sp, "tp": tp},
        device_id_type=MESH,
    )


def greet(peers):
    barrier = pltpu.get_barrier_semaphore()
    for sp, tp in peers:
        pl.semaphore_signal(
            barrier, inc=1, device_id={"sp": sp, "tp": tp}, device_id_type=MESH
        )
    pl.semaphore_wait(barrier, len(peers))


def when(condition, action):
    if condition is True:
        action()
    elif condition is not False:
        pl.when(condition)(action)


def spread_kernel(
    outer, inner, width,
    k, v, wg, wu, wd,
    kg, vg, gg, ug, dg,
    kv_up, kv_across, w_out_sem, w_across, recv, own_sem,
):
    s, t = lax.axis_index("sp"), lax.axis_index("tp")
    z, i = s // inner, s % inner
    units = wg.shape[1]
    greet(
        [((z + d) % outer * inner + i, t) for d in range(1, outer)]
        + [(z * inner + (i + e) % inner, t) for e in range(1, inner)]
    )

    def start_of(m):
        return pl.multiple_of(jnp.minimum(m * width, units - width), LANES)

    def weights(m):
        cut = pl.ds(start_of(m), width)
        return (wg.at[:, cut], wu.at[:, cut], wd.at[cut, :])

    pairs = ((k, kg), (v, vg))
    slots = (gg, ug, dg)

    def arrived(ref, slot, kind):
        remote(ref.at[slot], ref.at[slot], own_sem.at[0], recv.at[kind, slot], s, t).wait_recv()

    up_copies, across_copies, weight_copies, forward_copies = [], [], [], []
    for a in range(outer):
        slot = (z - a) * inner + i
        for kind, (mine, held) in enumerate(pairs):
            src = mine if a == 0 else held.at[slot]
            up = remote(
                src, held.at[slot], kv_up.at[kind, a], recv.at[kind, slot], s + inner, t
            )
            across = [
                (
                    remote(
                        src, held.at[slot], kv_across.at[kind, a, e], recv.at[kind, slot],
                        z * inner + (i + e) % inner, t,
                    ),
                    ((i + e) % inner > i) if a == 0 else (z >= a),
                )
                for e in range(1, inner)
            ]
            if a > 0:
                pl.when(z >= a)(lambda held=held, slot=slot, kind=kind: arrived(held, slot, kind))
            go_up = jnp.logical_and(z >= a, z + 1 < outer)
            pl.when(go_up)(up.start)
            for copy, needed in across:
                pl.when(needed)(copy.start)
            up_copies.append((up, go_up))
            across_copies += across
        if a == 0:
            own = [
                pltpu.make_async_copy(src, dst.at[s], own_sem.at[n])
                for n, (src, dst) in enumerate(
                    tuple(pairs) + tuple(zip(weights(z), slots))
                )
            ]
            for copy in own:
                copy.start()
            for d in range(1, outer):
                target = (z + d) % outer
                for kind, (src, held) in enumerate(zip(weights(target), slots)):
                    copy = remote(
                        src, held.at[s], w_out_sem.at[kind, d], recv.at[kind + 2, s],
                        target * inner + i, t,
                    )
                    copy.start()
                    weight_copies.append(copy)
        origin = (z + outer - a) % outer * inner + i
        for kind, (src, held) in enumerate(zip(weights(z), slots)):
            if a > 0:
                arrived(held, origin, kind + 2)
                src = held.at[origin]
            for e in range(1, inner):
                copy = remote(
                    src, held.at[origin], w_across.at[kind, a, e], recv.at[kind + 2, origin],
                    z * inner + (i + e) % inner, t,
                )
                copy.start()
                forward_copies.append(copy)
    for e in range(1, inner):
        other = (i + e) % inner
        for a in range(outer):
            slot = (z - a) * inner + other
            for kind, (mine, held) in enumerate(pairs):
                pl.when((other < i) if a == 0 else (z >= a))(
                    lambda held=held, slot=slot, kind=kind: arrived(held, slot, kind)
                )
            for kind, held in enumerate(slots):
                arrived(held, (z + outer - a) % outer * inner + other, kind + 2)
    for copy, needed in up_copies + across_copies:
        pl.when(needed)(copy.wait_send)
    for copy in weight_copies + forward_copies:
        copy.wait_send()
    for copy in own:
        copy.wait()


def spread(keys, values, w_gate, w_up, w_down, count, outer, width):
    inner = count // outer
    rows, units = w_gate.shape
    columns = w_down.shape[1]
    vmem, hbm = pl.BlockSpec(memory_space=pltpu.VMEM), pl.BlockSpec(memory_space=pl.ANY)
    kind = keys.dtype
    return pl.pallas_call(
        functools.partial(spread_kernel, outer, inner, width),
        out_shape=[
            jax.ShapeDtypeStruct((count,) + keys.shape, kind),
            jax.ShapeDtypeStruct((count,) + values.shape, kind),
            jax.ShapeDtypeStruct((count, rows, width), kind),
            jax.ShapeDtypeStruct((count, rows, width), kind),
            jax.ShapeDtypeStruct((count, width, columns), kind),
        ],
        in_specs=[vmem] * 5,
        out_specs=[hbm] * 5,
        scratch_shapes=[
            pltpu.SemaphoreType.DMA((2, outer)),
            pltpu.SemaphoreType.DMA((2, outer, inner)),
            pltpu.SemaphoreType.DMA((3, outer)),
            pltpu.SemaphoreType.DMA((3, outer, inner)),
            pltpu.SemaphoreType.DMA((5, count)),
            pltpu.SemaphoreType.DMA((5,)),
        ],
        compiler_params=pltpu.CompilerParams(collective_id=0, has_side_effects=True),
    )(keys, values, w_gate, w_up, w_down)


def attend_kernel(
    head_count, place, head_lambda, head_gain, q, kg, vg, w_out, out, row_max, weight_sum, acc, heads
):
    rows = q.shape[0]
    head_dim = q.shape[1] // (2 * head_count)
    value_dim = vg.shape[2] // head_count
    scale = head_dim ** (-0.5)
    row_max[...] = jnp.full_like(row_max, -1e30)
    weight_sum[...] = jnp.zeros_like(weight_sum)
    acc[...] = jnp.zeros_like(acc)

    def block(j, diagonal):
        for unit in range(2 * head_count):
            head = unit // 2
            columns = slice(unit * head_dim, (unit + 1) * head_dim)
            scores = (
                lax.dot_general(
                    q[:, columns], kg[j, :, columns], (((1,), (1,)), ((), ())),
                    preferred_element_type=jnp.float32,
                )
                * scale
            )
            if diagonal:
                seen = lax.broadcasted_iota(jnp.int32, scores.shape, 1) <= (
                    lax.broadcasted_iota(jnp.int32, scores.shape, 0)
                )
                scores = jnp.where(seen, scores, -1e30)
            old = row_max[unit]
            new = jnp.maximum(old, jnp.max(scores, axis=-1, keepdims=True))
            weights = jnp.exp(scores - new)
            if diagonal:
                weights = jnp.where(seen, weights, 0.0)
            fade = jnp.exp(old - new)
            row_max[unit] = new
            weight_sum[unit] = fade * weight_sum[unit] + jnp.sum(weights, axis=-1, keepdims=True)
            acc[unit] = fade * acc[unit] + jnp.dot(
                weights.astype(jnp.bfloat16),
                vg[j, :, head * value_dim : (head + 1) * value_dim],
                preferred_element_type=jnp.float32,
            )

    own = place[0]
    block(own, True)
    lax.fori_loop(0, own, lambda j, c: (block(j, False), c)[1], 0)
    for head in range(head_count):
        first = acc[2 * head] / weight_sum[2 * head]
        second = acc[2 * head + 1] / weight_sum[2 * head + 1]
        contrast = first - head_lambda[head] * second
        mean = jnp.mean(contrast * contrast, axis=-1, keepdims=True)
        heads[:, head * value_dim : (head + 1) * value_dim] = (
            contrast * lax.rsqrt(mean + epsilon) * head_gain[...]
        ).astype(jnp.bfloat16)
    out[...] = jnp.dot(heads[...], w_out[...], preferred_element_type=jnp.float32).astype(out.dtype)


def attend(place, head_lambda, head_gain, queries, kg, vg, w_out):
    head_count = head_lambda.shape[0]
    rows = queries.shape[0]
    value_dim = vg.shape[2] // head_count
    vmem, smem = pl.BlockSpec(memory_space=pltpu.VMEM), pl.BlockSpec(memory_space=pltpu.SMEM)
    units = 2 * head_count
    return pl.pallas_call(
        functools.partial(attend_kernel, head_count),
        out_shape=jax.ShapeDtypeStruct((rows, w_out.shape[1]), jnp.bfloat16),
        in_specs=[smem, smem] + [vmem] * 5,
        out_specs=vmem,
        scratch_shapes=[
            pltpu.VMEM((units, rows, 1), jnp.float32),
            pltpu.VMEM((units, rows, 1), jnp.float32),
            pltpu.VMEM((units, rows, value_dim), jnp.float32),
            pltpu.VMEM((rows, vg.shape[2]), jnp.bfloat16),
        ],
    )(place, head_lambda, head_gain.reshape(1, -1), queries, kg, vg, w_out)


def middle_kernel(
    outer, inner, high, low,
    projected, stream, gain, middle, gathered,
    parts, mine, first_send, first_recv, line_send, high_send, low_send, recv, own_sem,
):
    s, t = lax.axis_index("sp"), lax.axis_index("tp")
    z, i = s // inner, s % inner
    hi, lo = t // low, t % low
    tp = high * low
    rows = stream.shape[0]
    greet(
        [(s, (t + d) % tp) for d in range(1, tp)]
        + [((z + d) % outer * inner + i, t) for d in range(1, outer)]
    )
    first = []
    for d in range(1, tp):
        peer = (t + d) % tp
        copy = remote(
            projected.at[pl.ds(pl.multiple_of(peer * rows, rows), rows)], parts.at[t],
            first_send.at[d], first_recv.at[t], s, peer,
        )
        copy.start()
        first.append(copy)
    total = projected[pl.ds(pl.multiple_of(t * rows, rows), rows)].astype(jnp.float32)
    for d in range(1, tp):
        peer = (t + d) % tp
        remote(
            parts.at[peer], parts.at[peer], first_send.at[0], first_recv.at[peer], s, t
        ).wait_recv()
        total = total + parts[peer].astype(jnp.float32)
    total = total + stream[...].astype(jnp.float32)
    middle[...] = total
    mean = jnp.mean(total * total, axis=-1, keepdims=True)
    mine[...] = (total * lax.rsqrt(mean + epsilon) * gain[...]).astype(jnp.bfloat16)

    def arrived(zz, tt):
        remote(
            gathered.at[zz, tt], gathered.at[zz, tt], own_sem, recv.at[zz, tt], s, t
        ).wait_recv()

    copies = []
    for d in range(1, outer):
        copy = remote(
            mine, gathered.at[z, t], line_send.at[d], recv.at[z, t],
            (z + d) % outer * inner + i, t,
        )
        copy.start()
        copies.append(copy)
    own = pltpu.make_async_copy(mine, gathered.at[z, t], own_sem)
    own.start()
    for d in range(outer):
        zz = (z + outer - d) % outer
        if d > 0:
            arrived(zz, t)
        src = mine if d == 0 else gathered.at[zz, t]
        for e in range(1, high):
            copy = remote(
                src, gathered.at[zz, t], high_send.at[d, e], recv.at[zz, t],
                s, (hi + e) % high * low + lo,
            )
            copy.start()
            copies.append(copy)
        for f in range(1, low):
            copy = remote(
                src, gathered.at[zz, t], low_send.at[d, 0, f], recv.at[zz, t],
                s, hi * low + (lo + f) % low,
            )
            copy.start()
            copies.append(copy)
    for d in range(outer):
        zz = (z + outer - d) % outer
        for e in range(1, high):
            tt = (hi + e) % high * low + lo
            arrived(zz, tt)
            for f in range(1, low):
                copy = remote(
                    gathered.at[zz, tt], gathered.at[zz, tt], low_send.at[d, e, f],
                    recv.at[zz, tt], s, hi * low + (lo + f) % low,
                )
                copy.start()
                copies.append(copy)
    for d in range(outer):
        zz = (z + outer - d) % outer
        for e in range(high):
            for f in range(1, low):
                arrived(zz, (hi + e) % high * low + (lo + f) % low)
    for copy in first + copies:
        copy.wait_send()
    own.wait()


def middle_rows(projected, stream, gain, outer, inner, high, low):
    rows, width = stream.shape
    tp = high * low
    vmem = pl.BlockSpec(memory_space=pltpu.VMEM)
    dma = pltpu.SemaphoreType.DMA
    return pl.pallas_call(
        functools.partial(middle_kernel, outer, inner, high, low),
        out_shape=[
            jax.ShapeDtypeStruct((rows, width), jnp.float32),
            jax.ShapeDtypeStruct((outer, tp, rows, width), jnp.bfloat16),
        ],
        in_specs=[vmem] * 3,
        out_specs=[vmem] * 2,
        scratch_shapes=[
            pltpu.VMEM((tp, rows, width), jnp.bfloat16),
            pltpu.VMEM((rows, width), jnp.bfloat16),
            dma((tp,)),
            dma((tp,)),
            dma((outer,)),
            dma((outer, high)),
            dma((outer, high, low)),
            dma((outer, tp)),
            dma,
        ],
        compiler_params=pltpu.CompilerParams(collective_id=1, has_side_effects=True),
    )(projected, stream, gain.reshape(1, -1))


def reduce_kernel(
    outer, inner, high, low,
    partial, middle, out,
    in_low, in_high, in_line, sum_low, sum_high,
    low_send, low_recv, high_send, high_recv, line_send, line_recv,
):
    s, t = lax.axis_index("sp"), lax.axis_index("tp")
    z, i = s // inner, s % inner
    hi, lo = t // low, t % low
    greet(
        [(s, hi * low + (lo + f) % low) for f in range(1, low)]
        + [(s, (hi + e) % high * low + lo) for e in range(1, high)]
        + [((z + d) % outer * inner + i, t) for d in range(1, outer)]
    )
    order = [(z + d) % outer for d in range(1, outer + 1)]
    copies = []
    for d, zz in enumerate(order):
        for e in range(1, high + 1):
            hh = (hi + e) % high
            for f in range(1, low):
                other = (lo + f) % low
                copy = remote(
                    partial.at[zz, hh * low + other], in_low.at[f, zz, hh],
                    low_send.at[f, d, e % high], low_recv.at[f, zz, hh],
                    s, hi * low + other,
                )
                copy.start()
                copies.append(copy)
    for d, zz in enumerate(order):
        for e in range(1, high + 1):
            hh = (hi + e) % high
            total = partial[zz, hh * low + lo].astype(jnp.float32)
            for f in range(1, low):
                remote(
                    in_low.at[f, zz, hh], in_low.at[f, zz, hh], low_send.at[f, d, e % high],
                    low_recv.at[f, zz, hh], s, t,
                ).wait_recv()
                total = total + in_low[f, zz, hh].astype(jnp.float32)
            sum_low[zz, hh] = total.astype(jnp.bfloat16)
            if e < high:
                copy = remote(
                    sum_low.at[zz, hh], in_high.at[e, zz], high_send.at[e, d],
                    high_recv.at[e, zz], s, hh * low + lo,
                )
                copy.start()
                copies.append(copy)
    for d, zz in enumerate(order):
        total = sum_low[zz, hi].astype(jnp.float32)
        for e in range(1, high):
            remote(
                in_high.at[e, zz], in_high.at[e, zz], high_send.at[e, d],
                high_recv.at[e, zz], s, t,
            ).wait_recv()
            total = total + in_high[e, zz].astype(jnp.float32)
        if d + 1 < outer:
            sum_high[d] = total.astype(jnp.bfloat16)
            copy = remote(
                sum_high.at[d], in_line.at[d], line_send.at[d], line_recv.at[d],
                zz * inner + i, t,
            )
            copy.start()
            copies.append(copy)
    total = total + middle[...]
    for d in range(outer - 1):
        remote(
            in_line.at[d], in_line.at[d], line_send.at[d], line_recv.at[d], s, t
        ).wait_recv()
        total = total + in_line[d].astype(jnp.float32)
    out[...] = total.astype(out.dtype)
    for copy in copies:
        copy.wait_send()


def reduce_rows(partial, middle, outer, inner, high, low):
    rows, width = middle.shape
    vmem = pl.BlockSpec(memory_space=pltpu.VMEM)
    dma = pltpu.SemaphoreType.DMA
    kind = jnp.bfloat16
    return pl.pallas_call(
        functools.partial(reduce_kernel, outer, inner, high, low),
        out_shape=jax.ShapeDtypeStruct((rows, width), kind),
        in_specs=[vmem] * 2,
        out_specs=vmem,
        scratch_shapes=[
            pltpu.VMEM((low, outer, high, rows, width), kind),
            pltpu.VMEM((high, outer, rows, width), kind),
            pltpu.VMEM((outer, rows, width), kind),
            pltpu.VMEM((outer, high, rows, width), kind),
            pltpu.VMEM((outer, rows, width), kind),
            dma((low, outer, high)),
            dma((low, outer, high)),
            dma((high, outer)),
            dma((high, outer)),
            dma((outer,)),
            dma((outer,)),
        ],
        compiler_params=pltpu.CompilerParams(collective_id=2, has_side_effects=True),
    )(partial, middle)


def largest_part(count, limit):
    return max(part for part in range(1, limit + 1) if count % part == 0)


def shards(
    count, tp,
    stream, queries, keys, values, head_lambda, head_gain, w_out, norm_gain, w_gate, w_up, w_down,
):
    outer = largest_part(count, 4)
    inner = count // outer
    low = largest_part(tp, 2)
    high = tp // low
    units = w_gate.shape[1]
    width = -(-units // (LANES * outer)) * LANES
    rows, model = stream.shape
    s = lax.axis_index("sp")
    place = s.astype(jnp.int32).reshape(1)
    kg, vg, gg, ug, dg = spread(keys, values, w_gate, w_up, w_down, count, outer, width)
    projected = attend(place, head_lambda, head_gain, queries, kg, vg, w_out)
    middle, gathered = middle_rows(projected, stream, norm_gain, outer, inner, high, low)
    normed = gathered.reshape(-1, model)
    gate = jnp.dot(normed, gg.reshape(-1, width), preferred_element_type=jnp.float32)
    up_part = jnp.dot(normed, ug.reshape(-1, width), preferred_element_type=jnp.float32)
    hidden = (jax.nn.silu(gate) * up_part).astype(jnp.bfloat16)
    begin = (s // inner) * width
    repeated = begin - jnp.minimum(begin, units - width)
    hidden = jnp.where(jnp.arange(width)[None, :] >= repeated, hidden, 0).astype(jnp.bfloat16)
    down = dg.transpose(1, 0, 2).reshape(width, -1)
    partial = jnp.dot(hidden, down, preferred_element_type=jnp.float32).astype(jnp.bfloat16)
    return reduce_rows(
        partial.reshape(outer, tp, rows, model), middle, outer, inner, high, low
    )


def solution(mesh):
    placed = (
        P(("sp", "tp"), None),
        P("sp", "tp"),
        P("sp", "tp"),
        P("sp", "tp"),
        P("tp"),
        P(),
        P("tp", None),
        P(),
        P("sp", "tp"),
        P("sp", "tp"),
        P("tp", "sp"),
    )
    return jax.shard_map(
        functools.partial(shards, mesh.shape["sp"], mesh.shape["tp"]),
        mesh=mesh,
        in_specs=placed,
        out_specs=P(("sp", "tp"), None),
        check_vma=False,
    )
```

time: 500 us -> 238 us (0.48)
  waiting for transfers between devices: 434 us -> 0 us
  Pallas kernels: 0 us -> 221 us
  matrix products: 30.9 us -> 14.2 us
  between operations: 13.6 us -> 0.05 us
  other arithmetic: 10.6 us -> 0.01 us
  local copies, waits for them, and re-layouts: 10.4 us -> 2.53 us
    all_gather x6 -> x0, waiting for transfers between devices: 374 us -> none  [the longest x1 93.4 us: shards(): down_full = lax.all_gather(w_down, 'sp', axis=1, tiled=True)]
    pallas_call x0 -> x4, Pallas kernels: none -> 221 us  [the longest x1 101 us: middle_rows(): pl.pallas_call(functools.partial(middle_kernel, outer, inner, high, low),...]
    psum x1 -> x0, waiting for transfers between devices: 32.8 us -> none  [shards(): lax.psum(jnp.dot(head_out, w_out, preferred_element_type=jnp.float32).ast...]
    reduce_scatter x1 -> x0, waiting for transfers between devices: 23.1 us -> none  [shards(): lax.psum_scatter(jnp.dot(hidden, down_full, preferred_element_type=jnp.fl...]
    dot_general x5 -> x2, matrix products: 30.9 us -> 14.2 us  [the longest x1 7.85 us: shards(): jnp.dot(hidden, down, preferred_element_type=jnp.float32)]
    reshape x3 -> x0, local copies, waits for them, and re-layouts: 8.28 us -> none  [the longest x1 4.21 us: update(): key_heads = key_piece.reshape(span, head_count, 2, head_dim)]
  transfers between devices with their start and end apart: 8 -> 0, of which waited for: 7 -> 0; matrix products, arithmetic and copies ran while one was open for 8% -> 0% of each run, Pallas kernels for 0% -> 0%
where the time goes in v1:
time: 238 us; the launch traced here: 237 us
  Pallas kernels  221 us (93%)
  matrix products  14.2 us (6%)
  local copies, waits for them, and re-layouts  2.53 us (1%)
    pallas_call x1, Pallas kernels, middle_rows(): pl.pallas_call(functools.partial(middle_kernel, outer, inner, high, low),...  101 us
    pallas_call x1, Pallas kernels, spread(): pl.pallas_call(functools.partial(spread_kernel, outer, inner, width), out...  69.6 us
    pallas_call x1, Pallas kernels, reduce_rows(): pl.pallas_call(functools.partial(reduce_kernel, outer, inner, high, low),...  42.1 us
    dot_general x1, matrix products, shards(): jnp.dot(hidden, down, preferred_element_type=jnp.float32)  7.85 us
    pallas_call x1, Pallas kernels, attend(): pl.pallas_call(functools.partial(attend_kernel, head_count), out_shape=ja...  7.39 us
    dot_general x1, matrix products, shards(): jnp.dot(normed, gg.reshape(-1, width), preferred_element_type=jnp.float32)  6.34 us

profile of v1, /device:TPU:0, one launch (start us, length us, event | category | flops | bytes accessed | tf_op | source)
XLA Modules:
  0.0 237.4 jit_solution(3686743144602531913)
XLA Ops:
  0.0 69.6 %shard_map.109 = (bf16[8,256,512]{2,1,0:T(8,128)(2,1)}, bf16[8,256,512]{2,1,0:T(8,128)(2,1)}, bf16[8,256,384]{2,1,0:T(8,128)(2,1)}, bf16[8,256,384]{2,1,0:T(8,128)(2,1)}, bf16[8,384,256]{2,1,0:T(8,128)(2,1)}) custom-call(bf16[256,512]{1,0:T(8,128)(2,1)} %k.1, bf16[256,512]{1,0:T(8,128)(2,1)} %v.1, bf16[256,1408]{1,0:T(8,128)(2,1)} %wg.1, ...), custom_call_target="tpu_custom_call" | custom-call | tf_op jit(solution)/shard_map/pallas_call | solution.py:149
  69.6 0.0 copy-start
  69.6 7.4 %shard_map.110.projected = bf16[256,2048]{1,0:T(8,128)(2,1)} custom-call(s32[1]{0:T(128)} %bitcast.place, f32[2]{0:T(128)} %head_lambda.1, f32[1,256]{1,0:T(1,128)} %bitcast.18, bf16[256,512]{1,0:T(8,128)(2,1)} %q.1, bf16[8,256,512]{2,1,0:T(8,128)(2,1)} %get-tuple-element.12.kg, bf16[8,256,512]{2,1,0:T(8,128)(2,1)} %get-tuple-element.13.vg, ...), custom_call_target="tpu_custom_call" | custom-call | tf_op jit(solution)/shard_map/pallas_call | solution.py:233
  77.0 0.0 copy-done
  77.0 0.8 copy.12
  77.9 101.5 %shard_map.111 = (f32[64,2048]{1,0:T(8,128)}, bf16[4,4,64,2048]{3,2,1,0:T(8,128)(2,1)}) custom-call(bf16[256,2048]{1,0:T(8,128)(2,1)} %shard_map.110.projected, bf16[64,2048]{1,0:T(8,128)(2,1)} %stream.1, f32[1,2048]{1,0:T(1,128)} %bitcast.17), custom_call_target="tpu_custom_call" | custom-call | tf_op jit(solution)/shard_map/pallas_call | solution.py:343
  179.4 0.0 copy-start.1
  179.4 6.3 %fusion.6 = f32[1024,384]{1,0:T(8,128)} fusion(bf16[1024,2048]{1,0:T(8,128)(2,1)} %bitcast.19, bf16[2048,384]{1,0:T(8,128)(2,1)} %bitcast.22), kind=kOutput, calls=%fused_computation.9 | convolution fusion | flops 1610612736 | bytes 7340032 | tf_op jit(solution)/shard_map/dot_general | solution.py:487
  185.7 0.0 copy-done.1
  185.7 7.8 %convolution_convert_fusion = bf16[1024,2048]{1,0:T(8,128)(2,1)} fusion(bf16[384,2048]{0,1:T(8,128)(2,1)S(1)} %bitcast.15, bf16[1024,2048]{1,0:T(8,128)(2,1)} %bitcast.20, bf16[2048,384]{1,0:T(8,128)(2,1)S(1)} %bitcast.21, f32[1024,384]{1,0:T(8,128)} %fusion.6, pred[384]{0:T(512)(128)(4,1)S(1)} %iota_compare_fusion), kind=kOutput, calls=%fused_computation | convolution fusion | flops 3226075136 | bytes 13107584 | tf_op jit(solution)/shard_map/dot_general | solution.py:494
  193.6 42.1 %shard_map.112 = bf16[64,2048]{1,0:T(8,128)(2,1)} custom-call(bf16[4,4,64,2048]{3,2,1,0:T(8,128)(2,1)} %bitcast.14, f32[64,2048]{1,0:T(8,128)} %get-tuple-element.18.middle), custom_call_target="tpu_custom_call" | custom-call | tf_op jit(solution)/shard_map/pallas_call | solution.py:444
  235.7 1.7 copy.14
  (1 shorter events, 0.0 us)
Async XLA Ops:
  69.6 7.4 %copy-start = (bf16[8,384,256]{2,1,0:T(8,128)(2,1)S(1)}, bf16[8,384,256]{2,1,0:T(8,128)(2,1)}, u32[]{:S(2)}) copy-start(bf16[8,384,256]{2,1,0:T(8,128)(2,1)} %get-tuple-element.17) | copy-start | bytes 4718596
  179.4 6.4 %copy-start.1 = (bf16[8,256,384]{2,1,0:T(8,128)(2,1)S(1)}, bf16[8,256,384]{2,1,0:T(8,128)(2,1)}, u32[]{:S(2)}) copy-start(bf16[8,256,384]{2,1,0:T(8,128)(2,1)} %get-tuple-element.16) | copy-start | bytes 4718596

commit v2 on v1

v2 whole, which is shorter than its diff:
```python
import functools

import jax
import jax.numpy as jnp
from jax import lax
from jax.experimental import pallas as pl
from jax.experimental.pallas import tpu as pltpu
from jax.sharding import PartitionSpec as P

epsilon = 1e-06
MESH = pl.DeviceIdType.MESH
LANES = 128


def remote(src, dst, send_sem, recv_sem, sp, tp):
    return pltpu.make_async_remote_copy(
        src_ref=src,
        dst_ref=dst,
        send_sem=send_sem,
        recv_sem=recv_sem,
        device_id={"sp": sp, "tp": tp},
        device_id_type=MESH,
    )


def greet(peers):
    barrier = pltpu.get_barrier_semaphore()
    for sp, tp in peers:
        pl.semaphore_signal(
            barrier, inc=1, device_id={"sp": sp, "tp": tp}, device_id_type=MESH
        )
    pl.semaphore_wait(barrier, len(peers))


def when(condition, action):
    if condition is True:
        action()
    elif condition is not False:
        pl.when(condition)(action)


def front_kernel(
    outer, inner, high, low, width, head_count,
    head_lambda, head_gain, stream, q, k, v, w_out, gain, wg, wu, wd,
    middle, gathered, gg, ug, dg,
    kg, vg, row_max, weight_sum, acc, heads, projected, parts, mine,
    kv_up, kv_across, kv_recv, w_send, w_across, w_recv, own_sem,
    first_send, first_recv, line_send, high_send, low_send, recv,
):
    s, t = lax.axis_index("sp"), lax.axis_index("tp")
    z, i = s // inner, s % inner
    hi, lo = t // low, t % low
    tp = high * low
    units = wg.shape[1]
    rows = stream.shape[0]
    head_dim = q.shape[1] // (2 * head_count)
    value_dim = v.shape[1] // head_count
    scale = head_dim ** (-0.5)
    greet(
        [((z + d) % outer * inner + i, t) for d in range(1, outer)]
        + [(z * inner + (i + e) % inner, t) for e in range(1, inner)]
        + [(s, (t + d) % tp) for d in range(1, tp)]
    )

    def start_of(m):
        return pl.multiple_of(jnp.minimum(m * width, units - width), LANES)

    def weights(m):
        cut = pl.ds(start_of(m), width)
        return (wg.at[:, cut], wu.at[:, cut], wd.at[cut, :])

    pairs = ((k, kg), (v, vg))
    slots = (gg, ug, dg)
    sent = []

    def kv_arrived(slot):
        for kind, (mine_, held) in enumerate(pairs):
            remote(
                held.at[slot], held.at[slot], kv_up.at[0, 0], kv_recv.at[kind, slot], s, t
            ).wait_recv()

    def weights_arrived(slot):
        for kind, held in enumerate(slots):
            remote(
                held.at[slot], held.at[slot], w_send.at[0, 0], w_recv.at[kind, slot], s, t
            ).wait_recv()

    def send(copy, needed):
        if needed is True:
            copy.start()
        else:
            pl.when(needed)(copy.start)
        sent.append((copy, needed))

    def pass_kv(a):
        slot = (z - a) * inner + i
        for kind, (own_block, held) in enumerate(pairs):
            src = own_block if a == 0 else held.at[slot]
            send(
                remote(src, held.at[slot], kv_up.at[kind, a], kv_recv.at[kind, slot], s + inner, t),
                jnp.logical_and(z >= a, z + 1 < outer),
            )
            for e in range(1, inner):
                other = (i + e) % inner
                send(
                    remote(
                        src, held.at[slot], kv_across.at[kind, a, e], kv_recv.at[kind, slot],
                        z * inner + other, t,
                    ),
                    (other > i) if a == 0 else (z >= a),
                )

    def send_weights(offset):
        target = z + offset
        for kind, (src, held) in enumerate(zip(weights(target), slots)):
            send(
                remote(
                    src, held.at[s], w_send.at[kind, outer + offset], w_recv.at[kind, s],
                    target * inner + i, t,
                ),
                (target >= 0) if offset < 0 else (target < outer),
            )

    def forward_weights(offset):
        origin = (z + offset) * inner + i
        needed = True
        if offset:
            needed = (z + offset >= 0) if offset < 0 else (z + offset < outer)
            pl.when(needed)(lambda: weights_arrived(origin))
        for kind, (src, held) in enumerate(zip(weights(z), slots)):
            for e in range(1, inner):
                send(
                    remote(
                        held.at[origin] if offset else src, held.at[origin],
                        w_across.at[kind, outer + offset, e], w_recv.at[kind, origin],
                        z * inner + (i + e) % inner, t,
                    ),
                    needed,
                )

    def block(k_block, v_block, diagonal):
        for unit in range(2 * head_count):
            head = unit // 2
            columns = slice(unit * head_dim, (unit + 1) * head_dim)
            scores = (
                lax.dot_general(
                    q[:, columns], k_block[:, columns], (((1,), (1,)), ((), ())),
                    preferred_element_type=jnp.float32,
                )
                * scale
            )
            if diagonal:
                seen = lax.broadcasted_iota(jnp.int32, scores.shape, 1) <= (
                    lax.broadcasted_iota(jnp.int32, scores.shape, 0)
                )
                scores = jnp.where(seen, scores, -1e30)
            top = jnp.max(scores, axis=-1, keepdims=True)
            new = top if diagonal else jnp.maximum(row_max[unit], top)
            weights_ = jnp.exp(scores - new)
            if diagonal:
                weights_ = jnp.where(seen, weights_, 0.0)
            total = jnp.sum(weights_, axis=-1, keepdims=True)
            added = jnp.dot(
                weights_.astype(jnp.bfloat16),
                v_block[:, head * value_dim : (head + 1) * value_dim],
                preferred_element_type=jnp.float32,
            )
            if diagonal:
                weight_sum[unit] = total
                acc[unit] = added
            else:
                fade = jnp.exp(row_max[unit] - new)
                weight_sum[unit] = fade * weight_sum[unit] + total
                acc[unit] = fade * acc[unit] + added
            row_max[unit] = new

    pass_kv(0)
    own = [
        pltpu.make_async_copy(src, dst.at[s], own_sem.at[n])
        for n, (src, dst) in enumerate(zip(weights(z), slots))
    ]
    for copy in own:
        copy.start()
    for d in range(1, outer):
        send_weights(-d)
    forward_weights(0)
    block(k, v, True)
    for a in range(1, outer):
        slot = (z - a) * inner + i
        pl.when(z >= a)(lambda slot=slot: kv_arrived(slot))
        pass_kv(a)
        pl.when(z >= a)(lambda slot=slot: block(kg.at[slot], vg.at[slot], False))
    for d in range(1, outer):
        send_weights(d)
    for a in range(outer):
        for e in range(1, inner):
            other = (i + e) % inner
            slot = (z - a) * inner + other

            def take(slot=slot):
                kv_arrived(slot)
                block(kg.at[slot], vg.at[slot], False)

            pl.when((other < i) if a == 0 else (z >= a))(take)
    for head in range(head_count):
        contrast = (
            acc[2 * head] / weight_sum[2 * head]
            - head_lambda[head] * (acc[2 * head + 1] / weight_sum[2 * head + 1])
        )
        mean = jnp.mean(contrast * contrast, axis=-1, keepdims=True)
        heads[:, head * value_dim : (head + 1) * value_dim] = (
            contrast * lax.rsqrt(mean + epsilon) * head_gain[...]
        ).astype(jnp.bfloat16)
    projected[...] = jnp.dot(
        heads[...], w_out[...], preferred_element_type=jnp.float32
    ).astype(projected.dtype)

    for d in range(1, tp):
        peer = (t + d) % tp
        send(
            remote(
                projected.at[pl.ds(pl.multiple_of(peer * rows, rows), rows)], parts.at[t],
                first_send.at[d], first_recv.at[t], s, peer,
            ),
            True,
        )
    for d in range(1, outer):
        forward_weights(d)
    total = projected[pl.ds(pl.multiple_of(t * rows, rows), rows)].astype(jnp.float32)
    for d in range(1, tp):
        peer = (t + d) % tp
        remote(
            parts.at[peer], parts.at[peer], first_send.at[0], first_recv.at[peer], s, t
        ).wait_recv()
        total = total + parts[peer].astype(jnp.float32)
    total = total + stream[...].astype(jnp.float32)
    middle[...] = total
    mean = jnp.mean(total * total, axis=-1, keepdims=True)
    mine[...] = (total * lax.rsqrt(mean + epsilon) * gain[...]).astype(jnp.bfloat16)

    def arrived(zz, tt):
        remote(
            gathered.at[zz, tt], gathered.at[zz, tt], first_send.at[0], recv.at[zz, tt], s, t
        ).wait_recv()

    def pass_rows(d):
        zz = (z + outer - d) % outer
        src = mine if d == 0 else gathered.at[zz, t]
        for e in range(1, high):
            send(
                remote(
                    src, gathered.at[zz, t], high_send.at[d, e], recv.at[zz, t],
                    s, (hi + e) % high * low + lo,
                ),
                True,
            )
        for f in range(1, low):
            send(
                remote(
                    src, gathered.at[zz, t], low_send.at[d, 0, f], recv.at[zz, t],
                    s, hi * low + (lo + f) % low,
                ),
                True,
            )

    for d in range(1, outer):
        send(
            remote(
                mine, gathered.at[z, t], line_send.at[d], recv.at[z, t],
                (z + d) % outer * inner + i, t,
            ),
            True,
        )
    own_rows = pltpu.make_async_copy(mine, gathered.at[z, t], own_sem.at[3])
    own_rows.start()
    pass_rows(0)
    for d in range(1, outer):
        forward_weights(-d)
    for d in range(1, outer):
        arrived((z + outer - d) % outer, t)
        pass_rows(d)
    for d in range(outer):
        zz = (z + outer - d) % outer
        for e in range(1, high):
            tt = (hi + e) % high * low + lo
            arrived(zz, tt)
            for f in range(1, low):
                send(
                    remote(
                        gathered.at[zz, tt], gathered.at[zz, tt], low_send.at[d, e, f],
                        recv.at[zz, tt], s, hi * low + (lo + f) % low,
                    ),
                    True,
                )
    for d in range(outer):
        for e in range(high):
            for f in range(1, low):
                arrived((z + outer - d) % outer, (hi + e) % high * low + (lo + f) % low)
    for e in range(1, inner):
        for a in range(outer):
            weights_arrived((z + outer - a) % outer * inner + (i + e) % inner)
    for copy, needed in sent:
        if needed is True:
            copy.wait_send()
        else:
            pl.when(needed)(copy.wait_send)
    for copy in own + [own_rows]:
        copy.wait()


def front(
    stream, queries, keys, values, head_lambda, head_gain, w_out, norm_gain, w_gate, w_up, w_down,
    outer, inner, high, low, width,
):
    count, tp = outer * inner, high * low
    depth = w_gate.shape[0]
    columns = w_down.shape[1]
    rows, model = stream.shape
    tokens = queries.shape[0]
    head_count = head_lambda.shape[0]
    value_dim = values.shape[1] // head_count
    vmem, hbm = pl.BlockSpec(memory_space=pltpu.VMEM), pl.BlockSpec(memory_space=pl.ANY)
    smem = pl.BlockSpec(memory_space=pltpu.SMEM)
    dma = pltpu.SemaphoreType.DMA
    kind = jnp.bfloat16
    return pl.pallas_call(
        functools.partial(front_kernel, outer, inner, high, low, width, head_count),
        out_shape=[
            jax.ShapeDtypeStruct((rows, model), jnp.float32),
            jax.ShapeDtypeStruct((outer, tp, rows, model), kind),
            jax.ShapeDtypeStruct((count, depth, width), kind),
            jax.ShapeDtypeStruct((count, depth, width), kind),
            jax.ShapeDtypeStruct((count, width, columns), kind),
        ],
        in_specs=[smem] + [vmem] * 10,
        out_specs=[vmem, vmem, hbm, hbm, hbm],
        scratch_shapes=[
            pltpu.VMEM((count,) + keys.shape, kind),
            pltpu.VMEM((count,) + values.shape, kind),
            pltpu.VMEM((2 * head_count, tokens, 1), jnp.float32),
            pltpu.VMEM((2 * head_count, tokens, 1), jnp.float32),
            pltpu.VMEM((2 * head_count, tokens, value_dim), jnp.float32),
            pltpu.VMEM((tokens, values.shape[1]), kind),
            pltpu.VMEM((tokens, model), kind),
            pltpu.VMEM((tp, rows, model), kind),
            pltpu.VMEM((rows, model), kind),
            dma((2, outer)),
            dma((2, outer, inner)),
            dma((2, count)),
            dma((3, 2 * outer)),
            dma((3, 2 * outer, inner)),
            dma((3, count)),
            dma((4,)),
            dma((tp,)),
            dma((tp,)),
            dma((outer,)),
            dma((outer, high)),
            dma((outer, high, low)),
            dma((outer, tp)),
        ],
        compiler_params=pltpu.CompilerParams(collective_id=0, has_side_effects=True),
    )(
        head_lambda, head_gain.reshape(1, -1), stream, queries, keys, values, w_out,
        norm_gain.reshape(1, -1), w_gate, w_up, w_down,
    )


def back_kernel(
    outer, inner, high, low, units,
    normed, wg, wu, wd, middle, out,
    partial, in_low, in_high, in_line, sum_low, sum_high,
    low_send, low_recv, high_send, high_recv, line_send, line_recv,
):
    s, t = lax.axis_index("sp"), lax.axis_index("tp")
    z, i = s // inner, s % inner
    hi, lo = t // low, t % low
    tp = high * low
    rows, model = middle.shape
    width = wg.shape[1]
    greet(
        [(s, hi * low + (lo + f) % low) for f in range(1, low)]
        + [(s, (hi + e) % high * low + lo) for e in range(1, high)]
        + [((z + d) % outer * inner + i, t) for d in range(1, outer)]
    )
    repeated = z * width - jnp.minimum(z * width, units - width)
    copies = []

    def start(copy):
        copy.start()
        copies.append(copy)

    def compute(d):
        zz = (z + d + 1) % outer
        chunk = normed[zz].reshape(tp * rows, model)
        gate = jnp.dot(chunk, wg[...], preferred_element_type=jnp.float32)
        up_part = jnp.dot(chunk, wu[...], preferred_element_type=jnp.float32)
        hidden = gate / (1.0 + jnp.exp(-gate)) * up_part
        mine = lax.broadcasted_iota(jnp.int32, hidden.shape, 1) >= repeated
        hidden = jnp.where(mine, hidden, 0.0).astype(jnp.bfloat16)
        partial[zz] = (
            jnp.dot(hidden, wd[...], preferred_element_type=jnp.float32)
            .astype(partial.dtype)
            .reshape(tp, rows, model)
        )
        for e in range(1, high + 1):
            hh = (hi + e) % high
            for f in range(1, low):
                other = (lo + f) % low
                start(
                    remote(
                        partial.at[zz, hh * low + other], in_low.at[f, zz, hh],
                        low_send.at[f, d, e % high], low_recv.at[f, zz, hh],
                        s, hi * low + other,
                    )
                )

    def add_low(d):
        zz = (z + d + 1) % outer
        for e in range(1, high + 1):
            hh = (hi + e) % high
            total = partial[zz, hh * low + lo].astype(jnp.float32)
            for f in range(1, low):
                remote(
                    in_low.at[f, zz, hh], in_low.at[f, zz, hh], low_send.at[f, d, e % high],
                    low_recv.at[f, zz, hh], s, t,
                ).wait_recv()
                total = total + in_low[f, zz, hh].astype(jnp.float32)
            sum_low[zz, hh] = total.astype(jnp.bfloat16)
            if e < high:
                start(
                    remote(
                        sum_low.at[zz, hh], in_high.at[e, zz], high_send.at[e, d],
                        high_recv.at[e, zz], s, hh * low + lo,
                    )
                )

    def add_high(d):
        zz = (z + d + 1) % outer
        total = sum_low[zz, hi].astype(jnp.float32)
        for e in range(1, high):
            remote(
                in_high.at[e, zz], in_high.at[e, zz], high_send.at[e, d],
                high_recv.at[e, zz], s, t,
            ).wait_recv()
            total = total + in_high[e, zz].astype(jnp.float32)
        if d + 1 < outer:
            sum_high[d] = total.astype(jnp.bfloat16)
            start(
                remote(
                    sum_high.at[d], in_line.at[d], line_send.at[d], line_recv.at[d],
                    zz * inner + i, t,
                )
            )
        return total

    for step in range(outer + 2):
        if step < outer:
            compute(step)
        if 0 <= step - 1 < outer:
            add_low(step - 1)
        if 0 <= step - 2 < outer:
            total = add_high(step - 2)
    total = total + middle[...]
    for d in range(outer - 1):
        remote(
            in_line.at[d], in_line.at[d], line_send.at[d], line_recv.at[d], s, t
        ).wait_recv()
        total = total + in_line[d].astype(jnp.float32)
    out[...] = total.astype(out.dtype)
    for copy in copies:
        copy.wait_send()


def back(gathered, w_gate, w_up, w_down, middle, outer, inner, high, low, units):
    rows, width = middle.shape
    vmem = pl.BlockSpec(memory_space=pltpu.VMEM)
    dma = pltpu.SemaphoreType.DMA
    kind = jnp.bfloat16
    return pl.pallas_call(
        functools.partial(back_kernel, outer, inner, high, low, units),
        out_shape=jax.ShapeDtypeStruct((rows, width), kind),
        in_specs=[vmem] * 5,
        out_specs=vmem,
        scratch_shapes=[
            pltpu.VMEM((outer, high * low, rows, width), kind),
            pltpu.VMEM((low, outer, high, rows, width), kind),
            pltpu.VMEM((high, outer, rows, width), kind),
            pltpu.VMEM((outer, rows, width), kind),
            pltpu.VMEM((outer, high, rows, width), kind),
            pltpu.VMEM((outer, rows, width), kind),
            dma((low, outer, high)),
            dma((low, outer, high)),
            dma((high, outer)),
            dma((high, outer)),
            dma((outer,)),
            dma((outer,)),
        ],
        compiler_params=pltpu.CompilerParams(collective_id=2, has_side_effects=True),
    )(gathered, w_gate, w_up, w_down, middle)


def largest_part(count, limit):
    return max(part for part in range(1, limit + 1) if count % part == 0)


def shards(
    count, tp,
    stream, queries, keys, values, head_lambda, head_gain, w_out, norm_gain, w_gate, w_up, w_down,
):
    outer = largest_part(count, 4)
    inner = count // outer
    low = largest_part(tp, 2)
    high = tp // low
    units = w_gate.shape[1]
    width = -(-units // (LANES * outer)) * LANES
    middle, gathered, gg, ug, dg = front(
        stream, queries, keys, values, head_lambda, head_gain, w_out, norm_gain,
        w_gate, w_up, w_down, outer, inner, high, low, width,
    )
    down = dg.transpose(1, 0, 2).reshape(width, -1)
    return back(
        gathered, gg.reshape(-1, width), ug.reshape(-1, width), down, middle,
        outer, inner, high, low, units,
    )


def solution(mesh):
    placed = (
        P(("sp", "tp"), None),
        P("sp", "tp"),
        P("sp", "tp"),
        P("sp", "tp"),
        P("tp"),
        P(),
        P("tp", None),
        P(),
        P("sp", "tp"),
        P("sp", "tp"),
        P("tp", "sp"),
    )
    return jax.shard_map(
        functools.partial(shards, mesh.shape["sp"], mesh.shape["tp"]),
        mesh=mesh,
        in_specs=placed,
        out_specs=P(("sp", "tp"), None),
        check_vma=False,
    )
```

time: 238 us -> 178 us (0.75)
  Pallas kernels: 221 us -> 173 us
  matrix products: 14.2 us -> 0 us
    pallas_call x4 -> x2, Pallas kernels: 221 us -> 173 us  [the longest x1 117 us: front(): pl.pallas_call(functools.partial(front_kernel, outer, inner, high, low, w...]
    dot_general x2 -> x0, matrix products: 14.2 us -> none  [the longest x1 7.85 us: shards(): jnp.dot(hidden, down, preferred_element_type=jnp.float32)]
    reshape x0 -> x1, local copies, waits for them, and re-layouts: none -> 2.84 us  [shards(): down = dg.transpose(1, 0, 2).reshape(width, -1)]
where the time goes in v2:
time: 178 us
  Pallas kernels  173 us (97%)
  local copies, waits for them, and re-layouts  4.51 us (3%)
    pallas_call x1, Pallas kernels, front(): pl.pallas_call(functools.partial(front_kernel, outer, inner, high, low, w...  117 us
    pallas_call x1, Pallas kernels, back(): pl.pallas_call(functools.partial(back_kernel, outer, inner, high, low, un...  55.9 us

profile of v2, /device:TPU:0, one launch (start us, length us, event | category | flops | bytes accessed | tf_op | source)
XLA Modules:
  0.0 177.8 jit_solution(10222210188331696163)
XLA Ops:
  0.0 117.4 %shard_map.109 = (f32[64,2048]{1,0:T(8,128)}, bf16[4,4,64,2048]{3,2,1,0:T(8,128)(2,1)}, bf16[8,256,384]{2,1,0:T(8,128)(2,1)}, bf16[8,256,384]{2,1,0:T(8,128)(2,1)}, bf16[8,384,256]{2,1,0:T(8,128)(2,1)}) custom-call(f32[2]{0:T(128)} %head_lambda.1, f32[1,256]{1,0:T(1,128)} %bitcast.12, bf16[64,2048]{1,0:T(8,128)(2,1)} %stream.1, bf16[256,512]{1,0:T(8,128)(2,1)} %q.1, ...), custom_call_target="tpu_custom_call" | custom-call | tf_op jit(solution)/shard_map/pallas_call | solution.py:326
  117.4 2.8 %copy.13 = bf16[8,48,8,256]{3,2,0,1:T(8,128)(2,1)} copy(bf16[8,48,8,256]{3,2,1,0:T(8,128)(2,1)} %bitcast.10) | data formatting | bytes 3145728 | tf_op jit(solution)/shard_map/reshape | solution.py:520
  120.2 55.9 %shard_map.110 = bf16[64,2048]{1,0:T(8,128)(2,1)} custom-call(bf16[4,4,64,2048]{3,2,1,0:T(8,128)(2,1)} %get-tuple-element.10.normed, bf16[2048,384]{1,0:T(8,128)(2,1)} %bitcast.8, bf16[2048,384]{1,0:T(8,128)(2,1)} %bitcast.9, bf16[384,2048]{1,0:T(8,128)(2,1)} %bitcast.7, f32[64,2048]{1,0:T(8,128)} %get-tuple-element.14.middle), custom_call_target="tpu_custom_call" | custom-call | tf_op jit(solution)/shard_map/pallas_call | solution.py:479
  176.1 1.7 copy.15
